TPU v7x, 512 devices: a whole 4x8x8 slice. The times are simulated.
512 devices in a mesh: sp: 32 (over z, x), tp: 16 (over y, core).
Axes of the slice: x: 4, y: 8, z: 8, core: 2. Of those that a mesh axis runs over, the one named last changes fastest.
Arguments:
- residual: bfloat16 [8192, 2048], P('sp', 'tp'), may hold values from -26 to 26
- queries: bfloat16 [2048, 8192], P('tp', 'sp'), may hold values from -6 to 6
- keys: bfloat16 [2048, 8192], P('tp', 'sp'), may hold values from -6 to 6
- values: bfloat16 [2048, 8192], P('tp', 'sp'), may hold values from -12 to 12
- forget_cache: float32 [32, 8192], P('tp', 'sp'), as said below
- out_weight: bfloat16 [2048, 2048], P('tp'), may hold values from -0.125 to 0.125
- norm_gain: float32 [2048], replicated, may hold values from 0.1 to 1.9
- routes: int32 [8192, 2], P('sp'), may hold values from 0 to 31, all different within a row; in each aligned block of 256 rows (0 to 255, 256 to 511, ...) at most 20 rows name the same one
- route_weight: float32 [8192, 2], P('sp'), may hold values from 0.2 to 1
- gate_weight: bfloat16 [32, 2048, 4096], P('sp', None, 'tp'), may hold values from -0.125 to 0.125
- up_weight: bfloat16 [32, 2048, 4096], P('sp', None, 'tp'), may hold values from -0.125 to 0.125
- down_weight: bfloat16 [32, 4096, 2048], P('sp', 'tp'), may hold values from -0.09375 to 0.09375
Outputs:
- updated: bfloat16 [8192, 2048], P('sp', 'tp')
Inputs may be any that keep to these rules, and one draw needn't show every extreme that they name: `routes`: each row names 2 different experts; within the 256 rows of one index of sp no expert is named by more than 20 rows, and in the rows of some index some expert is named by exactly 20. `forget_cache`: each head's row never rises from one position to the next.
All inputs are finite; a program needn't handle non-finite values.
Results may differ from a plain program's by a relative error of at most 0.013.
Values may be sent and summed in bfloat16 or wider, within the bound.
No kernel may reach another device: no remote copies, remote signals or barrier semaphores. Data moves between devices by JAX's collectives and lax.ppermute only.
A program may use at most 64 MiB of HBM per device.

v0:
```python
import jax
import jax.numpy as jnp
from jax import lax
from jax.sharding import Mesh
from jax.sharding import PartitionSpec as P

SP = ("sp_0", "sp_1")
norm_eps = 1e-06
masked_score = -1e30
key_span = 1024


def gathered_by_axis(shard, axes, dim):
    out = shard
    for number in range(len(axes) - 1, -1, -1):
        out = lax.all_gather(out, axes[number], axis=dim, tiled=True)
    return out


def cut_along(shard, dim, peers):
    before, after = (shard.shape[:dim], shard.shape[dim + 1 :])
    return jnp.moveaxis(shard.reshape(*before, peers, -1, *after), dim, 0)


def sum_at_owner(shard, axis, dim):
    peers = lax.axis_size(axis)
    pieces = lax.all_to_all(cut_along(shard, dim, peers), axis, 0, 0, tiled=True)
    return jnp.sum(pieces.astype(jnp.float32), axis=0)


def sent_to_all(shard, axis):
    copies = jnp.broadcast_to(shard, (lax.axis_size(axis), *shard.shape))
    return lax.all_to_all(copies, axis, split_axis=0, concat_axis=0, tiled=True)


def taken_together(shard, axis):
    return sent_to_all(shard, axis).sum(axis=0)


def shards(
    residual,
    queries,
    keys,
    values,
    forget_cache,
    out_weight,
    norm_gain,
    routes,
    route_weight,
    gate_weight,
    up_weight,
    down_weight,
):
    sp_count = lax.axis_size(SP)
    token_count, local_width = residual.shape
    model_width = norm_gain.shape[0]
    head_count = forget_cache.shape[0]
    head_width = queries.shape[0] // head_count
    first_token = lax.axis_index(SP) * token_count
    last_token = first_token + token_count - 1
    query_heads = queries.reshape(head_count, head_width, token_count)
    query_place = first_token + jnp.arange(token_count, dtype=jnp.int32)
    score_scale = head_width ** (-0.5)

    def attend_block(state_now, key_block, value_block, cache_block, key_first):
        running_peak, running_total, running_sum = state_now
        block_length = key_block.shape[1]
        key_heads = key_block.reshape(head_count, head_width, block_length)
        value_heads = value_block.reshape(head_count, head_width, block_length)
        scores = (
            jnp.einsum("hdq,hdk->hqk", query_heads, key_heads, preferred_element_type=jnp.float32)
            * score_scale
        )
        scores = scores + forget_cache[:, :, None] - cache_block[:, None, :]
        key_place = key_first + jnp.arange(block_length, dtype=jnp.int32)
        allowed = key_place[None, :] <= query_place[:, None]
        scores = jnp.where(allowed[None], scores, masked_score)
        new_peak = jnp.maximum(running_peak, jnp.max(scores, axis=2))
        weights = jnp.exp(scores - new_peak[:, :, None])
        shrink = jnp.exp(running_peak - new_peak)
        new_total = running_total * shrink + jnp.sum(weights, axis=2)
        new_sum = running_sum * shrink[:, None, :] + jnp.einsum(
            "hdk,hqk->hdq",
            value_heads,
            weights.astype(jnp.bfloat16),
            preferred_element_type=jnp.float32,
        )
        return (new_peak, new_total, new_sum)

    initial = (
        jnp.full((head_count, token_count), masked_score, jnp.float32),
        jnp.zeros((head_count, token_count), jnp.float32),
        jnp.zeros((head_count, head_width, token_count), jnp.float32),
    )
    key_part = gathered_by_axis(keys.astype(jnp.float32), SP, 1).astype(jnp.bfloat16)
    value_part = gathered_by_axis(values.astype(jnp.float32), SP, 1).astype(jnp.bfloat16)
    cache_part = gathered_by_axis(forget_cache, SP, 1)
    part_length = key_part.shape[1]
    block_length = key_span

    def one_block(block_index, state_in):
        start_column = block_index * block_length
        key_block = lax.dynamic_slice_in_dim(key_part, start_column, block_length, 1)
        value_block = lax.dynamic_slice_in_dim(value_part, start_column, block_length, 1)
        cache_block = lax.dynamic_slice_in_dim(cache_part, start_column, block_length, 1)
        return lax.cond(
            start_column <= last_token,
            lambda inner: attend_block(inner, key_block, value_block, cache_block, start_column),
            lambda inner: inner,
            state_in,
        )

    final_peak, final_total, final_sum = lax.fori_loop(
        0, part_length // block_length, one_block, initial
    )
    attended = (
        (final_sum / final_total[:, None, :])
        .astype(jnp.bfloat16)
        .reshape(head_count * head_width, token_count)
    )
    projected = lax.dot_general(
        attended, out_weight, (((0,), (0,)), ((), ())), preferred_element_type=jnp.float32
    )
    head_sum = sum_at_owner(projected.astype(jnp.bfloat16), "tp", 1)
    stream = (residual.astype(jnp.float32) + head_sum).astype(jnp.bfloat16)
    top_count = routes.shape[1]
    item_count = token_count * top_count
    capacity = max(2, token_count * top_count * 5 // (4 * sp_count))
    expert_of = routes.reshape(item_count)
    onehot = (expert_of[:, None] == jnp.arange(sp_count, dtype=jnp.int32)[None, :]).astype(
        jnp.int32
    )
    earlier = jnp.cumsum(onehot, axis=0) - onehot
    target = expert_of * capacity + jnp.sum(earlier * onehot, axis=1)
    matches = target[None, :] == jnp.arange(sp_count * capacity, dtype=jnp.int32)[:, None]
    filled = jnp.any(matches, axis=1)
    source_row = (
        jnp.sum(jnp.where(matches, jnp.arange(item_count, dtype=jnp.int32)[None, :], 0), axis=1)
        // top_count
    )
    local_rows = stream.astype(jnp.float32)
    squares = taken_together(jnp.sum(local_rows * local_rows, axis=1), "tp")
    row_scale = lax.rsqrt(squares / model_width + norm_eps)
    local_gain = lax.dynamic_slice_in_dim(
        norm_gain, lax.axis_index("tp") * local_width, local_width
    )
    normed = (local_rows * row_scale[:, None] * local_gain[None, :]).astype(jnp.bfloat16)
    taken_rows = jnp.take(normed, source_row, axis=0)
    taken_rows = jnp.where(filled[:, None], taken_rows, jnp.zeros((), normed.dtype))
    arrived = lax.all_gather(
        lax.all_to_all(
            taken_rows.reshape(sp_count, capacity, normed.shape[1]),
            SP,
            split_axis=0,
            concat_axis=0,
            tiled=True,
        ),
        "tp",
        axis=2,
        tiled=True,
    )
    source_count = arrived.shape[0]
    slot_count = arrived.shape[1]
    flat_rows = arrived.reshape(source_count * slot_count, model_width)
    gate_value = jnp.dot(flat_rows, gate_weight[0], preferred_element_type=jnp.float32)
    up_value = jnp.dot(flat_rows, up_weight[0], preferred_element_type=jnp.float32)
    hidden = (jax.nn.silu(gate_value) * up_value).astype(jnp.bfloat16)
    down_value = jnp.dot(hidden, down_weight[0], preferred_element_type=jnp.float32)
    summed = sum_at_owner(
        down_value.reshape(source_count, slot_count, model_width).astype(jnp.bfloat16), "tp", 2
    )
    expert_back = lax.all_to_all(
        summed.astype(jnp.bfloat16), SP, split_axis=0, concat_axis=0, tiled=True
    )
    back_rows = expert_back.reshape(sp_count * capacity, local_width)
    picked = (
        jnp.take(back_rows, target, axis=0).astype(jnp.float32)
        * route_weight.reshape(item_count)[:, None]
    )
    mixture = jnp.sum(picked.reshape(token_count, top_count, local_width), axis=1)
    return (stream.astype(jnp.float32) + mixture).astype(jnp.bfloat16)


def solution(mesh):
    finer = Mesh(mesh.devices.reshape(8, 4, mesh.shape["tp"]), ("sp_0", "sp_1", "tp"))
    in_specs = (
        P(SP, "tp"),
        P("tp", SP),
        P("tp", SP),
        P("tp", SP),
        P("tp", SP),
        P("tp", None),
        P(),
        P(SP, None),
        P(SP, None),
        P(SP, None, "tp"),
        P(SP, None, "tp"),
        P(SP, "tp", None),
    )
    out_specs = P(SP, "tp")
    return jax.shard_map(
        shards, mesh=finer, in_specs=in_specs, out_specs=out_specs, check_vma=False
    )
```

profile of v0, /device:TPU:24, one launch (start us, length us, event | category | flops | bytes accessed | tf_op | source)
XLA Modules:
  0.0 361.6 jit_solution(1007863958048043251)
XLA Ops:
  6.5 14.3 %all_gather.21 = bf16[128,1024]{1,0:T(8,128)(2,1)} all-gather(bf16[128,256]{1,0:T(8,128)(2,1)} %param.18), channel_id=1, replica_groups=mesh['sp_0'=8,'sp_1'=4,'tp'=16] {'sp_1'}, dimensions={1}, use_global_device_ids=true | all-gather | bytes 327680 | tf_op jit(solution)/shard_map/all_gather | solution.py:16
  20.9 13.2 %all_gather.25 = bf16[128,1024]{1,0:T(8,128)(2,1)} all-gather(bf16[128,256]{1,0:T(8,128)(2,1)} %param.19), channel_id=1, replica_groups=mesh['sp_0'=8,'sp_1'=4,'tp'=16] {'sp_1'}, dimensions={1}, use_global_device_ids=true | all-gather | bytes 327680 | tf_op jit(solution)/shard_map/all_gather | solution.py:16
  34.2 10.6 %all_gather.23 = f32[2,1024]{1,0:T(2,128)S(1)} all-gather(f32[2,256]{1,0:T(2,128)} %param.20), channel_id=1, replica_groups=mesh['sp_0'=8,'sp_1'=4,'tp'=16] {'sp_1'}, dimensions={1}, use_global_device_ids=true | all-gather | bytes 10240 | tf_op jit(solution)/shard_map/all_gather | solution.py:16
  44.8 31.0 %all_gather.24 = f32[2,8192]{1,0:T(2,128)S(1)} all-gather(f32[2,1024]{1,0:T(2,128)S(1)} %all_gather.23), channel_id=1, replica_groups=mesh['sp_0'=8,'sp_1'=4,'tp'=16] {'sp_0'}, dimensions={1}, use_global_device_ids=true | all-gather | bytes 73728 | tf_op jit(solution)/shard_map/all_gather | solution.py:16
  75.7 36.7 %all-gather.6.cloned.1.call-done = bf16[128,8192]{1,0:T(8,128)(2,1)} async-done(((bf16[128,1024]{1,0:T(8,128)(2,1)}), bf16[128,8192]{1,0:T(8,128)(2,1)}) %all-gather.6.cloned.1.call-update) | async-done | bytes 2097168 | tf_op jit(solution)/shard_map/all_gather | solution.py:16
  112.5 4.2 %while.18 = (s32[]{:T(128)}, f32[2,256]{1,0:T(2,128)S(1)}, f32[2,256]{1,0:T(2,128)S(1)}, f32[2,64,256]{2,1,0:T(8,128)S(1)}, s32[]{:T(128)}, /*index=5*/bf16[128,...) while((s32[]{:T(128)}, f32[2,256]{1,0:T(2,128)S(1)}, ...), condition=%wide.region_5.6_spmd.clone, body=%wide.region_0.5_spmd.clone.sunk | while | flops 139266304 | bytes 8788313 | solution.py:113
  112.5 3.8 %conditional.3 = ((f32[2,256]{1,0:T(2,128)S(1)}, f32[2,256]{1,0:T(2,128)S(1)}, f32[2,64,256]{2,1,0:T(8,128)S(1)})) conditional(s32[]{:T(128)} %convert_element_type.119, (f32[2,256]{1,0:T(2,128)S(1)}, f32[2,256]{1,0:T(2,128)S(1)}, f32[2,64,256]{2,1,0:T(8,128)S(1)}) %tuple.55, (s32[]{:T(128)}, s32[]{:T(128)}, bf16[128,8192]{1,0:T(8,128)(2,1)}, ...), branch_computations={%region_1.0_spmd, %region_2.4_spmd} | conditional | flops 139266304 | bytes 8787026 | solution.py:106
  112.5 1.1 constant_dynamic-slice_fusion
  113.7 0.2 broadcast_compare_fusion
  113.9 1.6 fusion.26
  115.5 0.3 fusion.3
  115.8 0.5 convolution_add_fusion
  116.7 0.5 fusion.7
  117.2 1.3 copy.95
  118.4 7.4 %all-to-all-start = ((bf16[16,256,128]{2,1,0:T(8,128)(2,1)}), bf16[16,256,128]{2,1,0:T(8,128)(2,1)S(1)}, u32[]{:S(2)}, u32[]{:S(2)}) async-start(bf16[16,256,128]{2,1,0:T(8,128)(2,1)} %bitcast.60), calls=%async_computation | async-start | bytes 2097152 | tf_op jit(solution)/shard_map/all_to_all | solution.py:27
  126.0 0.1 eq.39
  126.1 0.1 reshape.233
  126.3 1.2 reduce-window.6
  127.4 0.2 slice_reduce_fusion
  127.8 0.2 select_reduce_fusion
  128.2 0.2 fusion.8
  128.4 23.6 %all-to-all-done = bf16[16,256,128]{2,1,0:T(8,128)(2,1)S(1)} async-done(((bf16[16,256,128]{2,1,0:T(8,128)(2,1)}), bf16[16,256,128]{2,1,0:T(8,128)(2,1)S(1)}, u32[]{:S(2)}, u32[]{:S(2)}) %all-to-all-start) | async-done | bytes 1048608 | tf_op jit(solution)/shard_map/all_to_all | solution.py:27
  152.0 0.1 convert_reduce_fusion
  152.3 0.6 broadcast_in_dim.101
  152.9 5.2 %all-to-all-start.1 = ((f32[16,1,256]{2,1,0:T(1,128)}), f32[16,1,256]{2,1,0:T(1,128)S(1)}, u32[]{:S(2)}, u32[]{:S(2)}) async-start(f32[16,1,256]{2,1,0:T(1,128)} %broadcast_in_dim.101), calls=%async_computation.1 | async-start | bytes 32768 | tf_op jit(solution)/shard_map/all_to_all | solution.py:33
  158.3 0.8 dynamic_slice.42
  159.1 3.6 all-to-all-done.1
  162.8 2.0 gather_fusion
  164.8 0.3 select_select_fusion
  165.1 44.1 %all_to_all.26 = bf16[32,20,128]{2,1,0:T(8,128)(2,1)} all-to-all(bf16[32,20,128]{2,1,0:T(8,128)(2,1)S(1)} %select_select_fusion), channel_id=1, replica_groups=mesh['sp_0'=8,'sp_1'=4,'tp'=16] {'sp_0','sp_1'}, dimensions={0} | all-to-all | bytes 327680 | tf_op jit(solution)/shard_map/all_to_all | solution.py:151
  209.2 39.2 %all-gather.8.cloned.1.call-done = bf16[32,20,2048]{2,1,0:T(8,128)(2,1)} async-done(((bf16[32,20,128]{2,1,0:T(8,128)(2,1)}), bf16[32,20,2048]{2,1,0:T(8,128)(2,1)}) %all-gather.8.cloned.1.call-update) | async-done | bytes 2621456 | tf_op jit(solution)/shard_map/all_gather | solution.py:150
  248.5 5.2 %reshape.235 = bf16[640,2048]{1,0:T(8,128)(2,1)} reshape(bf16[32,20,2048]{2,1,0:T(8,128)(2,1)} %all-gather.8.cloned.1.call-done) | data formatting | bytes 5242880 | tf_op jit(solution)/shard_map/reshape | solution.py:164
  253.7 2.7 fusion.12
  256.5 0.8 fusion.9
  257.4 0.9 fusion.6
  258.3 2.2 copy.94
  260.5 6.4 %all-to-all-start.3 = ((bf16[16,32,20,128]{3,1,2,0:T(8,128)(2,1)}), bf16[16,32,20,128]{3,1,2,0:T(8,128)(2,1)}, u32[]{:S(2)}, u32[]{:S(2)}) async-start(bf16[16,32,20,128]{3,1,2,0:T(8,128)(2,1)} %bitcast.62), calls=%async_computation.3 | async-start | bytes 5242880 | tf_op jit(solution)/shard_map/all_to_all | solution.py:27
  266.9 0.1 reduce_sum.88
  267.2 0.1 mul.123
  267.4 0.2 copy.75
  267.8 59.1 %all-to-all-done.3 = bf16[16,32,20,128]{3,1,2,0:T(8,128)(2,1)} async-done(((bf16[16,32,20,128]{3,1,2,0:T(8,128)(2,1)}), bf16[16,32,20,128]{3,1,2,0:T(8,128)(2,1)}, u32[]{:S(2)}, u32[]{:S(2)}) %all-to-all-start.3) | async-done | bytes 2621472 | tf_op jit(solution)/shard_map/all_to_all | solution.py:27
  326.9 2.1 reduce_sum.94
  329.0 0.7 copy.80
  329.8 9.9 %all-to-all-start.4 = ((bf16[32,20,128]{2,1,0:T(8,128)(2,1)}), bf16[32,20,128]{2,1,0:T(8,128)(2,1)S(1)}, u32[]{:S(2)}, u32[]{:S(2)}) async-start(bf16[32,20,128]{2,1,0:T(8,128)(2,1)} %copy.80), calls=%async_computation.4 | async-start | bytes 393216 | tf_op jit(solution)/shard_map/all_to_all | solution.py:172
  339.7 11.8 %all-to-all-done.4 = bf16[32,20,128]{2,1,0:T(8,128)(2,1)S(1)} async-done(((bf16[32,20,128]{2,1,0:T(8,128)(2,1)}), bf16[32,20,128]{2,1,0:T(8,128)(2,1)S(1)}, u32[]{:S(2)}, u32[]{:S(2)}) %all-to-all-start.4) | async-done | bytes 163872 | tf_op jit(solution)/shard_map/all_to_all | solution.py:172
  351.6 1.3 gather_fusion.1
  353.0 1.5 multiply_reduce_fusion
  354.4 0.7 fusion.18
  (73 shorter events, 1.7 us)
Async XLA Ops:
  6.5 250.9 %copy-start = (bf16[1,256,2048]{2,1,0:T(8,128)(2,1)S(1)}, bf16[1,256,2048]{2,1,0:T(8,128)(2,1)}, u32[]{:S(2)}) copy-start(bf16[1,256,2048]{2,1,0:T(8,128)(2,1)} %param.27) | copy-start | bytes 3145732
  6.5 69.2 %all-gather.4.cloned.1.call-start = ((), (), s32[]{:S(2)}) async-start(), calls=%async_computation.5 | async-start | bytes 2359296 | tf_op jit(solution)/shard_map/all_gather | solution.py:16
  20.9 91.5 %all-gather.6.cloned.1.call-start = ((), (), s32[]{:S(2)}) async-start(), calls=%async_computation.6 | async-start | bytes 2359296 | tf_op jit(solution)/shard_map/all_gather | solution.py:16
  112.4 4.2 %copy-start.2 = (bf16[128,2048]{1,0:T(8,128)(2,1)S(1)}, bf16[128,2048]{1,0:T(8,128)(2,1)}, u32[]{:S(2)}) copy-start(bf16[128,2048]{1,0:T(8,128)(2,1)} %param.21) | copy-start | bytes 1572868
  117.2 8.7 %copy-start.4 = (s32[256,2]{0,1:T(2,128)S(1)}, s32[256,2]{0,1:T(2,128)}, u32[]{:S(2)}) copy-start(s32[256,2]{0,1:T(2,128)} %param.23) | copy-start | bytes 6148
  118.4 33.7 %copy-start.3 = (bf16[256,128]{1,0:T(8,128)(2,1)S(1)}, bf16[256,128]{1,0:T(8,128)(2,1)}, u32[]{:S(2)}) copy-start(bf16[256,128]{1,0:T(8,128)(2,1)} %param.16) | copy-start | bytes 196612
  118.4 33.6 %all-to-all-start = ((bf16[16,256,128]{2,1,0:T(8,128)(2,1)}), bf16[16,256,128]{2,1,0:T(8,128)(2,1)S(1)}, u32[]{:S(2)}, u32[]{:S(2)}) async-start(bf16[16,256,128]{2,1,0:T(8,128)(2,1)} %bitcast.60), calls=%async_computation | async-start | bytes 2097152 | tf_op jit(solution)/shard_map/all_to_all | solution.py:27
  152.9 9.7 %all-to-all-start.1 = ((f32[16,1,256]{2,1,0:T(1,128)}), f32[16,1,256]{2,1,0:T(1,128)S(1)}, u32[]{:S(2)}, u32[]{:S(2)}) async-start(f32[16,1,256]{2,1,0:T(1,128)} %broadcast_in_dim.101), calls=%async_computation.1 | async-start | bytes 32768 | tf_op jit(solution)/shard_map/all_to_all | solution.py:33
  158.1 90.4 %all-gather.8.cloned.1.call-start = ((), (), s32[]{:S(2)}) async-start(), calls=%async_computation.7 | async-start | bytes 3342336 | tf_op jit(solution)/shard_map/all_gather | solution.py:150
  209.2 44.4 %copy-start.6 = (bf16[1,2048,256]{2,1,0:T(8,128)(2,1)S(1)}, bf16[1,2048,256]{2,1,0:T(8,128)(2,1)}, u32[]{:S(2)}) copy-start(bf16[1,2048,256]{2,1,0:T(8,128)(2,1)} %param.25) | copy-start | bytes 3145732
  253.7 2.8 copy-start.1
  253.7 2.8 copy-start.7
  260.5 7.2 %copy-start.5 = (f32[256,2]{0,1:T(2,128)S(1)}, f32[256,2]{0,1:T(2,128)}, u32[]{:S(2)}) copy-start(f32[256,2]{0,1:T(2,128)} %param.24) | copy-start | bytes 6148
  260.5 66.5 %all-to-all-start.3 = ((bf16[16,32,20,128]{3,1,2,0:T(8,128)(2,1)}), bf16[16,32,20,128]{3,1,2,0:T(8,128)(2,1)}, u32[]{:S(2)}, u32[]{:S(2)}) async-start(bf16[16,32,20,128]{3,1,2,0:T(8,128)(2,1)} %bitcast.62), calls=%async_computation.3 | async-start | bytes 5242880 | tf_op jit(solution)/shard_map/all_to_all | solution.py:27
  329.8 21.8 %all-to-all-start.4 = ((bf16[32,20,128]{2,1,0:T(8,128)(2,1)}), bf16[32,20,128]{2,1,0:T(8,128)(2,1)S(1)}, u32[]{:S(2)}, u32[]{:S(2)}) async-start(bf16[32,20,128]{2,1,0:T(8,128)(2,1)} %copy.80), calls=%async_computation.4 | async-start | bytes 393216 | tf_op jit(solution)/shard_map/all_to_all | solution.py:172
Sparse Core Ops, SparseCore 0:
  21.0 47.3 all-gather.3
  70.5 41.8 all-gather.5
  209.3 39.0 all-gather.7
where the time goes:
time: 363 us; the launch traced here: 362 us
  waiting for transfers between devices  174 us (48%)
  blocking collectives  113 us (31%)
  starting transfers between devices  29 us (8%)
  local copies, waits for them, and re-layouts  17.1 us (5%)
  between operations  13.4 us (4%)
  other arithmetic  7.3 us (2%)
  matrix products  6.94 us (2%)
    all_to_all x2, waiting for transfers between devices, sum_at_owner(): lax.all_to_all(cut_along(shard, dim, peers), axis, 0, 0, tiled=True)  82.8 us
    all_gather x4, blocking collectives, gathered_by_axis(): out = lax.all_gather(out, axes[number], axis=dim, tiled=True)  69.1 us
    all_to_all x1, blocking collectives, shards(): lax.all_to_all(taken_rows.reshape(sp_count, capacity, normed.shape[1]), S...  44.1 us
    all_gather x1, waiting for transfers between devices, shards(): lax.all_gather(lax.all_to_all(taken_rows.reshape(sp_count, capacity, norm...  39.2 us
    all_gather x2, waiting for transfers between devices, gathered_by_axis(): out = lax.all_gather(out, axes[number], axis=dim, tiled=True)  36.7 us
    all_to_all x2, starting transfers between devices, sum_at_owner(): lax.all_to_all(cut_along(shard, dim, peers), axis, 0, 0, tiled=True)  13.8 us
    all_to_all x1, waiting for transfers between devices, shards(): lax.all_to_all(summed.astype(jnp.bfloat16), SP, split_axis=0, concat_axis...  11.8 us
    all_to_all x1, starting transfers between devices, shards(): lax.all_to_all(summed.astype(jnp.bfloat16), SP, split_axis=0, concat_axis...  9.92 us
  transfers between devices with their start and end apart: 7, of which 6 were waited for; matrix products, arithmetic and copies ran while one was open for 1% of the time, Pallas kernels for 0%

commit v1 on v0

--- a/solution.py
+++ b/solution.py
@@ -147,18 +147,28 @@
     normed = (local_rows * row_scale[:, None] * local_gain[None, :]).astype(jnp.bfloat16)
     taken_rows = jnp.take(normed, source_row, axis=0)
     taken_rows = jnp.where(filled[:, None], taken_rows, jnp.zeros((), normed.dtype))
-    arrived = lax.all_gather(
-        lax.all_to_all(
-            taken_rows.reshape(sp_count, capacity, normed.shape[1]),
-            SP,
-            split_axis=0,
-            concat_axis=0,
-            tiled=True,
-        ),
-        "tp",
-        axis=2,
+    array = lax.all_to_all(
+        taken_rows.reshape(sp_count, capacity, normed.shape[1]),
+        SP,
+        split_axis=0,
+        concat_axis=0,
         tiled=True,
     )
+    ways, here, step = (lax.axis_size("tp"), lax.axis_index("tp"), array.shape[2])
+    shape = [n * ways if d == 2 else n for d, n in enumerate(array.shape)]
+    full = lax.dynamic_update_slice_in_dim(
+        jnp.zeros(shape, array.dtype), array, here * step, axis=2
+    )
+    going_up = going_down = array
+    for far in range(1, ways // 2 + 1):
+        going_up = lax.ppermute(going_up, "tp", [(d, (d + 1) % ways) for d in range(ways)])
+        full = lax.dynamic_update_slice_in_dim(full, going_up, (here - far) % ways * step, axis=2)
+        if 2 * far < ways:
+            going_down = lax.ppermute(going_down, "tp", [(d, (d - 1) % ways) for d in range(ways)])
+            full = lax.dynamic_update_slice_in_dim(
+                full, going_down, (here + far) % ways * step, axis=2
+            )
+    arrived = full
     source_count = arrived.shape[0]
     slot_count = arrived.shape[1]
     flat_rows = arrived.reshape(source_count * slot_count, model_width)

time: 363 us -> 370 us (1.019)
  waiting for transfers between devices: 174 us -> 144 us
  starting transfers between devices: 29 us -> 52.9 us
  local copies, waits for them, and re-layouts: 17.1 us -> 30.7 us
    all_gather x1 -> x0, waiting for transfers between devices: 39.2 us -> none  [shards(): lax.all_gather(lax.all_to_all(taken_rows.reshape(sp_count, capacity, norm...]
    ppermute x0 -> x15, starting transfers between devices: none -> 21.1 us  [the longest x8 14.8 us: shards(): lax.ppermute(going_up, 'tp', [(d, (d + 1) % ways) for d in range(ways)])]
    dynamic_update_slice x0 -> x16, local copies, waits for them, and re-layouts: none -> 11.6 us  [the longest x8 5.75 us: shards(): lax.dynamic_update_slice_in_dim(full, going_up, (here - far) % ways * ste...]
    all_to_all x2, starting transfers between devices: 13.8 us -> 22.6 us  [sum_at_owner(): lax.all_to_all(cut_along(shard, dim, peers), axis, 0, 0, tiled=True)]
    ppermute x0 -> x15, waiting for transfers between devices: none -> 8.61 us  [the longest x8 8.59 us: shards(): lax.ppermute(going_up, 'tp', [(d, (d + 1) % ways) for d in range(ways)])]
    all_to_all x1, starting transfers between devices: 9.92 us -> 3.86 us  [shards(): lax.all_to_all(summed.astype(jnp.bfloat16), SP, split_axis=0, concat_axis...]
  transfers between devices with their start and end apart: 7 -> 21, of which waited for: 6 -> 11; matrix products, arithmetic and copies ran while one was open for 1% -> 5% of each run, Pallas kernels for 0% -> 0%
where the time goes in v1:
time: 370 us; the launch traced here: 369 us
  waiting for transfers between devices  144 us (39%)
  blocking collectives  113 us (31%)
  starting transfers between devices  52.9 us (14%)
  local copies, waits for them, and re-layouts  30.7 us (8%)
  between operations  13.8 us (4%)
  other arithmetic  7.3 us (2%)
  matrix products  6.94 us (2%)
    all_to_all x2, waiting for transfers between devices, sum_at_owner(): lax.all_to_all(cut_along(shard, dim, peers), axis, 0, 0, tiled=True)  82.8 us
    all_gather x4, blocking collectives, gathered_by_axis(): out = lax.all_gather(out, axes[number], axis=dim, tiled=True)  69.1 us
    all_to_all x1, blocking collectives, shards(): lax.all_to_all(taken_rows.reshape(sp_count, capacity, normed.shape[1]), S...  44 us
    all_gather x2, waiting for transfers between devices, gathered_by_axis(): out = lax.all_gather(out, axes[number], axis=dim, tiled=True)  36.7 us
    all_to_all x2, starting transfers between devices, sum_at_owner(): lax.all_to_all(cut_along(shard, dim, peers), axis, 0, 0, tiled=True)  22.6 us
    ppermute x8, starting transfers between devices, shards(): lax.ppermute(going_up, 'tp', [(d, (d + 1) % ways) for d in range(ways)])  14.8 us
    all_to_all x1, waiting for transfers between devices, shards(): lax.all_to_all(summed.astype(jnp.bfloat16), SP, split_axis=0, concat_axis...  12.3 us
    ppermute x8, waiting for transfers between devices, shards(): lax.ppermute(going_up, 'tp', [(d, (d + 1) % ways) for d in range(ways)])  8.59 us
  transfers between devices with their start and end apart: 21, of which 11 were waited for; matrix products, arithmetic and copies ran while one was open for 5% of the time, Pallas kernels for 0%

profile of v1, /device:TPU:24, one launch (start us, length us, event | category | flops | bytes accessed | tf_op | source)
XLA Modules:
  0.0 369.1 jit_solution(2559893279427847043)
XLA Ops:
  6.5 14.3 %all_gather.18 = bf16[128,1024]{1,0:T(8,128)(2,1)} all-gather(bf16[128,256]{1,0:T(8,128)(2,1)} %param.18), channel_id=1, replica_groups=mesh['sp_0'=8,'sp_1'=4,'tp'=16] {'sp_1'}, dimensions={1}, use_global_device_ids=true | all-gather | bytes 327680 | tf_op jit(solution)/shard_map/all_gather | solution.py:16
  20.9 13.2 %all_gather.22 = bf16[128,1024]{1,0:T(8,128)(2,1)} all-gather(bf16[128,256]{1,0:T(8,128)(2,1)} %param.19), channel_id=1, replica_groups=mesh['sp_0'=8,'sp_1'=4,'tp'=16] {'sp_1'}, dimensions={1}, use_global_device_ids=true | all-gather | bytes 327680 | tf_op jit(solution)/shard_map/all_gather | solution.py:16
  34.2 10.6 %all_gather.20 = f32[2,1024]{1,0:T(2,128)S(1)} all-gather(f32[2,256]{1,0:T(2,128)} %param.20), channel_id=1, replica_groups=mesh['sp_0'=8,'sp_1'=4,'tp'=16] {'sp_1'}, dimensions={1}, use_global_device_ids=true | all-gather | bytes 10240 | tf_op jit(solution)/shard_map/all_gather | solution.py:16
  44.8 31.0 %all_gather.21 = f32[2,8192]{1,0:T(2,128)S(1)} all-gather(f32[2,1024]{1,0:T(2,128)S(1)} %all_gather.20), channel_id=1, replica_groups=mesh['sp_0'=8,'sp_1'=4,'tp'=16] {'sp_0'}, dimensions={1}, use_global_device_ids=true | all-gather | bytes 73728 | tf_op jit(solution)/shard_map/all_gather | solution.py:16
  75.8 36.7 %all-gather.5.cloned.1.call-done = bf16[128,8192]{1,0:T(8,128)(2,1)} async-done(((bf16[128,1024]{1,0:T(8,128)(2,1)}), bf16[128,8192]{1,0:T(8,128)(2,1)}) %all-gather.5.cloned.1.call-update) | async-done | bytes 2097168 | tf_op jit(solution)/shard_map/all_gather | solution.py:16
  112.5 4.2 %while.18 = (s32[]{:T(128)}, f32[2,256]{1,0:T(2,128)S(1)}, f32[2,256]{1,0:T(2,128)S(1)}, f32[2,64,256]{2,1,0:T(8,128)S(1)}, s32[]{:T(128)}, /*index=5*/bf16[128,...) while((s32[]{:T(128)}, f32[2,256]{1,0:T(2,128)S(1)}, ...), condition=%wide.region_5.6_spmd.clone, body=%wide.region_0.5_spmd.clone.sunk | while | flops 139266304 | bytes 8788313 | solution.py:113
  112.5 3.8 %conditional.3 = ((f32[2,256]{1,0:T(2,128)S(1)}, f32[2,256]{1,0:T(2,128)S(1)}, f32[2,64,256]{2,1,0:T(8,128)S(1)})) conditional(s32[]{:T(128)} %convert_element_type.119, (f32[2,256]{1,0:T(2,128)S(1)}, f32[2,256]{1,0:T(2,128)S(1)}, f32[2,64,256]{2,1,0:T(8,128)S(1)}) %tuple.55, (s32[]{:T(128)}, s32[]{:T(128)}, bf16[128,8192]{1,0:T(8,128)(2,1)}, ...), branch_computations={%region_1.0_spmd, %region_2.4_spmd} | conditional | flops 139266304 | bytes 8787026 | solution.py:106
  112.5 1.1 constant_dynamic-slice_fusion
  113.9 1.6 fusion.26
  117.2 1.2 copy.95
  118.4 7.3 %all-to-all-start = ((bf16[16,256,128]{2,1,0:T(8,128)(2,1)}), bf16[16,256,128]{2,1,0:T(8,128)(2,1)S(1)}, u32[]{:S(2)}, u32[]{:S(2)}) async-start(bf16[16,256,128]{2,1,0:T(8,128)(2,1)} %bitcast.62), calls=%async_computation | async-start | bytes 2097152 | tf_op jit(solution)/shard_map/all_to_all | solution.py:27
  126.1 1.2 reduce-window.6
  128.3 23.6 %all-to-all-done = bf16[16,256,128]{2,1,0:T(8,128)(2,1)S(1)} async-done(((bf16[16,256,128]{2,1,0:T(8,128)(2,1)}), bf16[16,256,128]{2,1,0:T(8,128)(2,1)S(1)}, u32[]{:S(2)}, u32[]{:S(2)}) %all-to-all-start) | async-done | bytes 1048608 | tf_op jit(solution)/shard_map/all_to_all | solution.py:27
  152.8 5.2 %all-to-all-start.1 = ((f32[16,1,256]{2,1,0:T(1,128)}), f32[16,1,256]{2,1,0:T(1,128)S(1)}, u32[]{:S(2)}, u32[]{:S(2)}) async-start(f32[16,1,256]{2,1,0:T(1,128)} %broadcast_in_dim.105), calls=%async_computation.1 | async-start | bytes 32768 | tf_op jit(solution)/shard_map/all_to_all | solution.py:33
  158.1 0.8 dynamic_slice.42
  158.9 3.6 all-to-all-done.1
  162.7 2.0 gather_fusion
  165.0 44.0 %all_to_all.26 = bf16[32,20,128]{2,1,0:T(8,128)(2,1)S(1)} all-to-all(bf16[32,20,128]{2,1,0:T(8,128)(2,1)S(1)} %select_select_fusion), channel_id=1, replica_groups=mesh['sp_0'=8,'sp_1'=4,'tp'=16] {'sp_0','sp_1'}, dimensions={0} | all-to-all | bytes 327680 | tf_op jit(solution)/shard_map/all_to_all | solution.py:150
  209.0 1.7 collective-permute-start.1
  210.7 2.0 broadcast_in_dim.99
  214.1 1.7 collective-permute-start.3
  216.5 0.7 constant_dynamic-update-slice_fusion.13
  217.3 1.9 collective-permute-done.2
  219.2 1.7 collective-permute-start.5
  221.6 0.7 constant_dynamic-update-slice_fusion.11
  222.4 1.9 collective-permute-done.4
  224.9 1.1 collective-permute-start.7
  227.4 1.9 collective-permute-done.6
  229.3 1.9 collective-permute-start.8
  232.7 1.8 collective-permute-done.8
  234.4 3.1 collective-permute-start.10
  239.5 4.3 %collective-permute-start.12 = (bf16[32,20,128]{2,1,0:T(8,128)(2,1)S(1)}, bf16[32,20,128]{2,1,0:T(8,128)(2,1)S(1)}, u32[]{:S(2)}, u32[]{:S(2)}) collective-permute-start(bf16[32,20,128]{2,1,0:T(8,128)(2,1)S(1)} %collective-permute-done.10), channel_id=1, source_target_pairs={{0,1},{1,2},{2,3},{3,4},{4,5},{5,6},{6,7},{7,8},{8,9},{9,10},{10,1... | collective-permute-start | bytes 491528 | tf_op jit(solution)/shard_map/ppermute | solution.py:164
  244.6 0.7 constant_dynamic-update-slice_fusion.3
  245.3 4.8 %collective-permute-start.14 = (bf16[32,20,128]{2,1,0:T(8,128)(2,1)S(1)}, bf16[32,20,128]{2,1,0:T(8,128)(2,1)S(1)}, u32[]{:S(2)}, u32[]{:S(2)}) collective-permute-start(bf16[32,20,128]{2,1,0:T(8,128)(2,1)S(1)} %collective-permute-done.12), channel_id=1, source_target_pairs={{0,1},{1,2},{2,3},{3,4},{4,5},{5,6},{6,7},{7,8},{8,9},{9,10},{10,1... | collective-permute-start | bytes 491528 | tf_op jit(solution)/shard_map/ppermute | solution.py:164
  250.9 0.7 constant_dynamic-update-slice_fusion.1
  252.3 5.2 %reshape.235 = bf16[640,2048]{1,0:T(8,128)(2,1)} reshape(bf16[32,20,2048]{2,1,0:T(8,128)(2,1)} %constant_dynamic-update-slice_fusion) | data formatting | bytes 5242880 | tf_op jit(solution)/shard_map/reshape | solution.py:174
  257.5 2.7 fusion.12
  260.3 0.8 multiply_convert_fusion
  261.3 0.8 fusion.6
  262.1 2.2 copy.94
  264.3 15.4 %all-to-all-start.3 = ((bf16[16,32,20,128]{3,1,2,0:T(8,128)(2,1)}), bf16[16,32,20,128]{3,1,2,0:T(8,128)(2,1)}, u32[]{:S(2)}, u32[]{:S(2)}) async-start(bf16[16,32,20,128]{3,1,2,0:T(8,128)(2,1)} %bitcast.64), calls=%async_computation.3 | async-start | bytes 5242880 | tf_op jit(solution)/shard_map/all_to_all | solution.py:27
  280.6 59.1 %all-to-all-done.3 = bf16[16,32,20,128]{3,1,2,0:T(8,128)(2,1)} async-done(((bf16[16,32,20,128]{3,1,2,0:T(8,128)(2,1)}), bf16[16,32,20,128]{3,1,2,0:T(8,128)(2,1)}, u32[]{:S(2)}, u32[]{:S(2)}) %all-to-all-start.3) | async-done | bytes 2621472 | tf_op jit(solution)/shard_map/all_to_all | solution.py:27
  339.7 2.1 reduce_sum.94
  341.8 0.7 copy.80
  342.6 3.9 %all-to-all-start.4 = ((bf16[32,20,128]{2,1,0:T(8,128)(2,1)}), bf16[32,20,128]{2,1,0:T(8,128)(2,1)S(1)}, u32[]{:S(2)}, u32[]{:S(2)}) async-start(bf16[32,20,128]{2,1,0:T(8,128)(2,1)} %copy.80), calls=%async_computation.4 | async-start | bytes 393216 | tf_op jit(solution)/shard_map/all_to_all | solution.py:182
  346.5 12.3 %all-to-all-done.4 = bf16[32,20,128]{2,1,0:T(8,128)(2,1)S(1)} async-done(((bf16[32,20,128]{2,1,0:T(8,128)(2,1)}), bf16[32,20,128]{2,1,0:T(8,128)(2,1)S(1)}, u32[]{:S(2)}, u32[]{:S(2)}) %all-to-all-start.4) | async-done | bytes 163872 | tf_op jit(solution)/shard_map/all_to_all | solution.py:182
  358.8 1.3 gather_fusion.1
  360.2 1.5 multiply_reduce_fusion
  (117 shorter events, 16.7 us)
Async XLA Ops:
  6.5 254.7 %copy-start = (bf16[1,256,2048]{2,1,0:T(8,128)(2,1)S(1)}, bf16[1,256,2048]{2,1,0:T(8,128)(2,1)}, u32[]{:S(2)}) copy-start(bf16[1,256,2048]{2,1,0:T(8,128)(2,1)} %param.27) | copy-start | bytes 3145732
  6.5 69.2 %all-gather.3.cloned.1.call-start = ((), (), s32[]{:S(2)}) async-start(), calls=%async_computation.5 | async-start | bytes 2359296 | tf_op jit(solution)/shard_map/all_gather | solution.py:16
  20.9 91.5 %all-gather.5.cloned.1.call-start = ((), (), s32[]{:S(2)}) async-start(), calls=%async_computation.6 | async-start | bytes 2359296 | tf_op jit(solution)/shard_map/all_gather | solution.py:16
  112.5 4.3 %copy-start.2 = (bf16[128,2048]{1,0:T(8,128)(2,1)S(1)}, bf16[128,2048]{1,0:T(8,128)(2,1)}, u32[]{:S(2)}) copy-start(bf16[128,2048]{1,0:T(8,128)(2,1)} %param.21) | copy-start | bytes 1572868
  116.7 9.0 %copy-start.4 = (s32[256,2]{0,1:T(2,128)S(1)}, s32[256,2]{0,1:T(2,128)}, u32[]{:S(2)}) copy-start(s32[256,2]{0,1:T(2,128)} %param.23) | copy-start | bytes 6148
  117.2 34.9 %copy-start.3 = (bf16[256,128]{1,0:T(8,128)(2,1)S(1)}, bf16[256,128]{1,0:T(8,128)(2,1)}, u32[]{:S(2)}) copy-start(bf16[256,128]{1,0:T(8,128)(2,1)} %param.16) | copy-start | bytes 196612
  118.4 33.5 %all-to-all-start = ((bf16[16,256,128]{2,1,0:T(8,128)(2,1)}), bf16[16,256,128]{2,1,0:T(8,128)(2,1)S(1)}, u32[]{:S(2)}, u32[]{:S(2)}) async-start(bf16[16,256,128]{2,1,0:T(8,128)(2,1)} %bitcast.62), calls=%async_computation | async-start | bytes 2097152 | tf_op jit(solution)/shard_map/all_to_all | solution.py:27
  152.8 9.7 %all-to-all-start.1 = ((f32[16,1,256]{2,1,0:T(1,128)}), f32[16,1,256]{2,1,0:T(1,128)S(1)}, u32[]{:S(2)}, u32[]{:S(2)}) async-start(f32[16,1,256]{2,1,0:T(1,128)} %broadcast_in_dim.105), calls=%async_computation.1 | async-start | bytes 32768 | tf_op jit(solution)/shard_map/all_to_all | solution.py:33
  209.0 5.1 %collective-permute-start = (bf16[32,20,128]{2,1,0:T(8,128)(2,1)S(1)}, bf16[32,20,128]{2,1,0:T(8,128)(2,1)S(1)}, u32[]{:S(2)}, u32[]{:S(2)}) collective-permute-start(bf16[32,20,128]{2,1,0:T(8,128)(2,1)S(1)} %all_to_all.26), channel_id=1, source_target_pairs={{0,1},{1,2},{2,3},{3,4},{4,5},{5,6},{6,7},{7,8},{8,9},{9,10},{10,1... | collective-permute-start | bytes 491528 | tf_op jit(solution)/shard_map/ppermute | solution.py:164
  209.0 5.1 %collective-permute-start.1 = (bf16[32,20,128]{2,1,0:T(8,128)(2,1)S(1)}, bf16[32,20,128]{2,1,0:T(8,128)(2,1)S(1)}, u32[]{:S(2)}, u32[]{:S(2)}) collective-permute-start(bf16[32,20,128]{2,1,0:T(8,128)(2,1)S(1)} %all_to_all.26), channel_id=1, source_target_pairs={{0,15},{1,0},{2,1},{3,2},{4,3},{5,4},{6,5},{7,6},{8,7},{9,8},{10,9... | collective-permute-start | bytes 491528 | tf_op jit(solution)/shard_map/ppermute | solution.py:167
  214.1 5.1 %collective-permute-start.2 = (bf16[32,20,128]{2,1,0:T(8,128)(2,1)S(1)}, bf16[32,20,128]{2,1,0:T(8,128)(2,1)S(1)}, u32[]{:S(2)}, u32[]{:S(2)}) collective-permute-start(bf16[32,20,128]{2,1,0:T(8,128)(2,1)S(1)} %collective-permute-done), channel_id=1, source_target_pairs={{0,1},{1,2},{2,3},{3,4},{4,5},{5,6},{6,7},{7,8},{8,9},{9,10},{10,1... | collective-permute-start | bytes 491528 | tf_op jit(solution)/shard_map/ppermute | solution.py:164
  214.1 5.1 %collective-permute-start.3 = (bf16[32,20,128]{2,1,0:T(8,128)(2,1)S(1)}, bf16[32,20,128]{2,1,0:T(8,128)(2,1)S(1)}, u32[]{:S(2)}, u32[]{:S(2)}) collective-permute-start(bf16[32,20,128]{2,1,0:T(8,128)(2,1)S(1)} %collective-permute-done.1), channel_id=1, source_target_pairs={{0,15},{1,0},{2,1},{3,2},{4,3},{5,4},{6,5},{7,6},{8,7},{9,8},{10,9... | collective-permute-start | bytes 491528 | tf_op jit(solution)/shard_map/ppermute | solution.py:167
  219.2 5.1 %collective-permute-start.4 = (bf16[32,20,128]{2,1,0:T(8,128)(2,1)S(1)}, bf16[32,20,128]{2,1,0:T(8,128)(2,1)S(1)}, u32[]{:S(2)}, u32[]{:S(2)}) collective-permute-start(bf16[32,20,128]{2,1,0:T(8,128)(2,1)S(1)} %collective-permute-done.2), channel_id=1, source_target_pairs={{0,1},{1,2},{2,3},{3,4},{4,5},{5,6},{6,7},{7,8},{8,9},{9,10},{10,1... | collective-permute-start | bytes 491528 | tf_op jit(solution)/shard_map/ppermute | solution.py:164
  219.2 5.8 %collective-permute-start.5 = (bf16[32,20,128]{2,1,0:T(8,128)(2,1)S(1)}, bf16[32,20,128]{2,1,0:T(8,128)(2,1)S(1)}, u32[]{:S(2)}, u32[]{:S(2)}) collective-permute-start(bf16[32,20,128]{2,1,0:T(8,128)(2,1)S(1)} %collective-permute-done.3), channel_id=1, source_target_pairs={{0,15},{1,0},{2,1},{3,2},{4,3},{5,4},{6,5},{7,6},{8,7},{9,8},{10,9... | collective-permute-start | bytes 491528 | tf_op jit(solution)/shard_map/ppermute | solution.py:167
  224.2 5.1 %collective-permute-start.6 = (bf16[32,20,128]{2,1,0:T(8,128)(2,1)S(1)}, bf16[32,20,128]{2,1,0:T(8,128)(2,1)S(1)}, u32[]{:S(2)}, u32[]{:S(2)}) collective-permute-start(bf16[32,20,128]{2,1,0:T(8,128)(2,1)S(1)} %collective-permute-done.4), channel_id=1, source_target_pairs={{0,1},{1,2},{2,3},{3,4},{4,5},{5,6},{6,7},{7,8},{8,9},{9,10},{10,1... | collective-permute-start | bytes 491528 | tf_op jit(solution)/shard_map/ppermute | solution.py:164
  224.9 6.3 %collective-permute-start.7 = (bf16[32,20,128]{2,1,0:T(8,128)(2,1)S(1)}, bf16[32,20,128]{2,1,0:T(8,128)(2,1)S(1)}, u32[]{:S(2)}, u32[]{:S(2)}) collective-permute-start(bf16[32,20,128]{2,1,0:T(8,128)(2,1)S(1)} %collective-permute-done.5), channel_id=1, source_target_pairs={{0,15},{1,0},{2,1},{3,2},{4,3},{5,4},{6,5},{7,6},{8,7},{9,8},{10,9... | collective-permute-start | bytes 491528 | tf_op jit(solution)/shard_map/ppermute | solution.py:167
  229.3 5.1 %collective-permute-start.8 = (bf16[32,20,128]{2,1,0:T(8,128)(2,1)S(1)}, bf16[32,20,128]{2,1,0:T(8,128)(2,1)S(1)}, u32[]{:S(2)}, u32[]{:S(2)}) collective-permute-start(bf16[32,20,128]{2,1,0:T(8,128)(2,1)S(1)} %collective-permute-done.6), channel_id=1, source_target_pairs={{0,1},{1,2},{2,3},{3,4},{4,5},{5,6},{6,7},{7,8},{8,9},{9,10},{10,1... | collective-permute-start | bytes 491528 | tf_op jit(solution)/shard_map/ppermute | solution.py:164
  231.2 6.3 %collective-permute-start.9 = (bf16[32,20,128]{2,1,0:T(8,128)(2,1)S(1)}, bf16[32,20,128]{2,1,0:T(8,128)(2,1)S(1)}, u32[]{:S(2)}, u32[]{:S(2)}) collective-permute-start(bf16[32,20,128]{2,1,0:T(8,128)(2,1)S(1)} %collective-permute-done.7), channel_id=1, source_target_pairs={{0,15},{1,0},{2,1},{3,2},{4,3},{5,4},{6,5},{7,6},{8,7},{9,8},{10,9... | collective-permute-start | bytes 491528 | tf_op jit(solution)/shard_map/ppermute | solution.py:167
  234.4 5.1 %collective-permute-start.10 = (bf16[32,20,128]{2,1,0:T(8,128)(2,1)S(1)}, bf16[32,20,128]{2,1,0:T(8,128)(2,1)S(1)}, u32[]{:S(2)}, u32[]{:S(2)}) collective-permute-start(bf16[32,20,128]{2,1,0:T(8,128)(2,1)S(1)} %collective-permute-done.8), channel_id=1, source_target_pairs={{0,1},{1,2},{2,3},{3,4},{4,5},{5,6},{6,7},{7,8},{8,9},{9,10},{10,1... | collective-permute-start | bytes 491528 | tf_op jit(solution)/shard_map/ppermute | solution.py:164
  237.5 6.3 %collective-permute-start.11 = (bf16[32,20,128]{2,1,0:T(8,128)(2,1)S(1)}, bf16[32,20,128]{2,1,0:T(8,128)(2,1)S(1)}, u32[]{:S(2)}, u32[]{:S(2)}) collective-permute-start(bf16[32,20,128]{2,1,0:T(8,128)(2,1)S(1)} %collective-permute-done.9), channel_id=1, source_target_pairs={{0,15},{1,0},{2,1},{3,2},{4,3},{5,4},{6,5},{7,6},{8,7},{9,8},{10,9... | collective-permute-start | bytes 491528 | tf_op jit(solution)/shard_map/ppermute | solution.py:167
  239.5 5.8 %collective-permute-start.12 = (bf16[32,20,128]{2,1,0:T(8,128)(2,1)S(1)}, bf16[32,20,128]{2,1,0:T(8,128)(2,1)S(1)}, u32[]{:S(2)}, u32[]{:S(2)}) collective-permute-start(bf16[32,20,128]{2,1,0:T(8,128)(2,1)S(1)} %collective-permute-done.10), channel_id=1, source_target_pairs={{0,1},{1,2},{2,3},{3,4},{4,5},{5,6},{6,7},{7,8},{8,9},{9,10},{10,1... | collective-permute-start | bytes 491528 | tf_op jit(solution)/shard_map/ppermute | solution.py:164
  243.8 7.0 %collective-permute-start.13 = (bf16[32,20,128]{2,1,0:T(8,128)(2,1)S(1)}, bf16[32,20,128]{2,1,0:T(8,128)(2,1)S(1)}, u32[]{:S(2)}, u32[]{:S(2)}) collective-permute-start(bf16[32,20,128]{2,1,0:T(8,128)(2,1)S(1)} %collective-permute-done.11), channel_id=1, source_target_pairs={{0,15},{1,0},{2,1},{3,2},{4,3},{5,4},{6,5},{7,6},{8,7},{9,8},{10,9... | collective-permute-start | bytes 491528 | tf_op jit(solution)/shard_map/ppermute | solution.py:167
  245.3 6.3 %collective-permute-start.14 = (bf16[32,20,128]{2,1,0:T(8,128)(2,1)S(1)}, bf16[32,20,128]{2,1,0:T(8,128)(2,1)S(1)}, u32[]{:S(2)}, u32[]{:S(2)}) collective-permute-start(bf16[32,20,128]{2,1,0:T(8,128)(2,1)S(1)} %collective-permute-done.12), channel_id=1, source_target_pairs={{0,1},{1,2},{2,3},{3,4},{4,5},{5,6},{6,7},{7,8},{8,9},{9,10},{10,1... | collective-permute-start | bytes 491528 | tf_op jit(solution)/shard_map/ppermute | solution.py:164
  251.6 5.9 %copy-start.6 = (bf16[1,2048,256]{2,1,0:T(8,128)(2,1)S(1)}, bf16[1,2048,256]{2,1,0:T(8,128)(2,1)}, u32[]{:S(2)}) copy-start(bf16[1,2048,256]{2,1,0:T(8,128)(2,1)} %param.25) | copy-start | bytes 3145732
  257.5 2.8 copy-start.1
  257.5 2.8 copy-start.7
  264.3 16.1 %copy-start.5 = (f32[256,2]{0,1:T(2,128)S(1)}, f32[256,2]{0,1:T(2,128)}, u32[]{:S(2)}) copy-start(f32[256,2]{0,1:T(2,128)} %param.24) | copy-start | bytes 6148
  264.3 75.4 %all-to-all-start.3 = ((bf16[16,32,20,128]{3,1,2,0:T(8,128)(2,1)}), bf16[16,32,20,128]{3,1,2,0:T(8,128)(2,1)}, u32[]{:S(2)}, u32[]{:S(2)}) async-start(bf16[16,32,20,128]{3,1,2,0:T(8,128)(2,1)} %bitcast.64), calls=%async_computation.3 | async-start | bytes 5242880 | tf_op jit(solution)/shard_map/all_to_all | solution.py:27
  342.6 16.2 %all-to-all-start.4 = ((bf16[32,20,128]{2,1,0:T(8,128)(2,1)}), bf16[32,20,128]{2,1,0:T(8,128)(2,1)S(1)}, u32[]{:S(2)}, u32[]{:S(2)}) async-start(bf16[32,20,128]{2,1,0:T(8,128)(2,1)} %copy.80), calls=%async_computation.4 | async-start | bytes 393216 | tf_op jit(solution)/shard_map/all_to_all | solution.py:182
Sparse Core Ops, SparseCore 0:
  21.0 47.3 all-gather.2
  70.4 41.9 all-gather.4
